TPU v7x, 32 devices: a whole 2x2x4 slice. The times are simulated.
32 devices in a mesh: row: 8 (over z, y), col: 4 (over x, core).
Axes of the slice: x: 2, y: 2, z: 4, core: 2. Of those that a mesh axis runs over, the one named last changes fastest.
Arguments:
- tokens: bfloat16 [4096, 2048], P('row'), may hold values from -6 to 6
- outer_weight: bfloat16 [2048, 1024], P(None, 'col'), may hold values from -0.125 to 0.125
- inner_weight: bfloat16 [2048, 1024], P(None, 'col'), may hold values from -0.125 to 0.125
- value_weight: bfloat16 [2048, 1024], P(None, 'col'), may hold values from -0.125 to 0.125
- conv_taps: float32 [3, 3, 1024], P(None, None, 'col'), may hold values from -3.5 to 3.5
- feature_weight: float32 [33, 128], replicated, may hold values from -1 to 1
- feature_phase: float32 [128], replicated, may hold values from -3.140625 to 3.140625
- inner_mats: float32 [2, 128, 128], replicated, may hold values from -0.5 to 0.5
- inner_phase: float32 [2, 128], replicated, may hold values from -3.140625 to 3.140625
- frequency: float32 [128], replicated, may hold values from 0.1 to 1.9
- forward_weight: float32 [128, 1024], P(None, 'col'), may hold values from -0.5 to 0.5
- backward_weight: float32 [128, 1024], P(None, 'col'), may hold values from -0.5 to 0.5
- decay_rate: float32 [1024], P('col'), may hold values from 0.2 to 409.6, as said below
- skip_gain: float32 [1024], P('col'), may hold values from -6 to 6
- output_weight: bfloat16 [1024, 2048], replicated, may hold values from -0.1875 to 0.1875
Outputs:
- layer_out: bfloat16 [4096, 2048], P(('row', 'col'))
Inputs may be any that keep to these rules, and one draw needn't show every extreme that they name: `decay_rate`: positive rates of the channels' filter windows.
All inputs are finite; a program needn't handle non-finite values.
Results may differ from a plain program's by a relative error of at most 0.014.
Values may be sent and summed in bfloat16 or wider, within the bound.
A program may use at most 64 MiB of HBM per device.

v0:
```python
import functools
import math

import jax
import jax.numpy as jnp
import numpy as np
from jax import lax
from jax.experimental import pallas as pl
from jax.experimental.pallas import tpu as pltpu
from jax.sharding import PartitionSpec as P

BANDS = 16
INNER = 2
FACTOR = 256


PRECISE = lax.Precision.HIGHEST


def with_halo(array, sides, width):
    for axis, dim in sides:
        devices, length = (lax.axis_size(axis), array.shape[dim])
        up = [(i, (i + 1) % devices) for i in range(devices - 1)]
        down = [(j, i) for i, j in up]
        last = lax.slice_in_dim(array, length - width, length, axis=dim)
        leading = lax.slice_in_dim(array, 0, width, axis=dim)
        before = lax.ppermute(last, axis, up)
        after = lax.ppermute(leading, axis, down)
        array = jnp.concatenate([before, array, after], axis=dim)
    return array


def phases(height, breadth, period):
    row_index = lax.broadcasted_iota(jnp.int32, (height, breadth), 0)
    col_index = lax.broadcasted_iota(jnp.int32, (height, breadth), 1)
    phase_angle = 2.0 * math.pi / period * (row_index * col_index % period).astype(jnp.float32)
    return (jnp.cos(phase_angle), jnp.sin(phase_angle))


def along_last(operand, matrix):
    return jnp.einsum("ckb,bj->ckj", operand, matrix, precision=PRECISE)


def forward_transform(operand, tables):
    cosine_one, sine_one, twist_cos, twist_sin, cosine_two, sine_two = tables
    used_rows = operand.shape[1]
    first_real = jnp.einsum("kr,crb->ckb", cosine_one[:, :used_rows], operand, precision=PRECISE)
    first_imag = -jnp.einsum("kr,crb->ckb", sine_one[:, :used_rows], operand, precision=PRECISE)
    turned_real = first_real * twist_cos + first_imag * twist_sin
    turned_imag = first_imag * twist_cos - first_real * twist_sin
    spec_real = along_last(turned_real, cosine_two) + along_last(turned_imag, sine_two)
    spec_imag = along_last(turned_imag, cosine_two) - along_last(turned_real, sine_two)
    return (spec_real, spec_imag)


def inverse_transform(spec_real, spec_imag, tables, kept_rows):
    cosine_one, sine_one, twist_cos, twist_sin, cosine_two, sine_two = tables
    back_real = along_last(spec_real, cosine_two) - along_last(spec_imag, sine_two)
    back_imag = along_last(spec_imag, cosine_two) + along_last(spec_real, sine_two)
    untwist_real = back_real * twist_cos - back_imag * twist_sin
    untwist_imag = back_imag * twist_cos + back_real * twist_sin
    return jnp.einsum(
        "nk,ckb->cnb", cosine_one[:kept_rows], untwist_real, precision=PRECISE
    ) - jnp.einsum("nk,ckb->cnb", sine_one[:kept_rows], untwist_imag, precision=PRECISE)


def position_filters(
    places,
    seq_length,
    feature_weight,
    feature_phase,
    inner_mats,
    inner_phase,
    frequency,
    forward_cols,
    backward_cols,
    rates,
):
    scaled = places.astype(jnp.float32) / (seq_length - 1)
    band_ints = 1 + jnp.arange(BANDS, dtype=jnp.int32) * (seq_length // (4 * BANDS))
    turns = places[:, None] * band_ints[None, :] % seq_length
    angles = 2.0 * math.pi / seq_length * turns.astype(jnp.float32)
    features = jnp.concatenate([scaled[:, None], jnp.cos(angles), -jnp.sin(angles)], axis=1)
    hidden = jnp.sin(
        frequency * (jnp.dot(features, feature_weight, precision=PRECISE) + feature_phase)
    )
    for level_index in range(INNER):
        hidden = jnp.sin(
            frequency
            * (
                jnp.dot(hidden, inner_mats[level_index], precision=PRECISE)
                + inner_phase[level_index]
            )
        )
    window = jnp.exp(-scaled[:, None] * rates[None, :])
    filter_ahead = jnp.dot(hidden, forward_cols, precision=PRECISE) * window
    filter_behind = jnp.dot(hidden, backward_cols, precision=PRECISE) * window
    return (filter_ahead, filter_behind)


def on_device(
    tokens,
    outer_weight,
    inner_weight,
    value_weight,
    conv_taps,
    feature_weight,
    feature_phase,
    inner_mats,
    inner_phase,
    frequency,
    forward_weight,
    backward_weight,
    decay_rate,
    skip_gain,
    output_weight,
):
    block_rows = tokens.shape[0]
    seq_length = block_rows * lax.axis_size("row")
    own_width = outer_weight.shape[1]
    outer_proj = jnp.dot(tokens, outer_weight, preferred_element_type=jnp.float32).astype(
        jnp.bfloat16
    )
    inner_proj = jnp.dot(tokens, inner_weight, preferred_element_type=jnp.float32).astype(
        jnp.bfloat16
    )
    value_proj = jnp.dot(tokens, value_weight, preferred_element_type=jnp.float32).astype(
        jnp.bfloat16
    )
    stacked = jnp.concatenate([outer_proj, inner_proj, value_proj], axis=1)
    padded = with_halo(stacked, (("row", 0),), 1).astype(jnp.float32)
    tap_table = conv_taps.reshape(3, 3 * own_width)
    convolved = padded[:-2] * tap_table[0] + padded[1:-1] * tap_table[1] + padded[2:] * tap_table[2]
    gate_part = convolved[:, :own_width].astype(jnp.bfloat16)
    signal = (convolved[:, own_width : 2 * own_width] * convolved[:, 2 * own_width :]).astype(
        jnp.bfloat16
    )
    offset = lax.axis_index("row") * block_rows
    places = offset + jnp.arange(block_rows, dtype=jnp.int32)
    filter_ahead, filter_behind = position_filters(
        places,
        seq_length,
        feature_weight,
        feature_phase,
        inner_mats,
        inner_phase,
        frequency,
        forward_weight,
        backward_weight,
        decay_rate,
    )
    moved_signal, moved_ahead, moved_behind = (
        lax.all_to_all(signal.astype(jnp.float32), "row", split_axis=1, concat_axis=0, tiled=True),
        lax.all_to_all(filter_ahead, "row", split_axis=1, concat_axis=0, tiled=True),
        lax.all_to_all(filter_behind, "row", split_axis=1, concat_axis=0, tiled=True),
    )
    per_device = moved_ahead.shape[1]
    ahead_rows = moved_ahead.T
    behind_rows = moved_behind.T
    norm_scale = lax.rsqrt(
        1.0
        + jnp.sum(jnp.square(ahead_rows), axis=1)
        + jnp.sum(jnp.square(behind_rows[:, 1:]), axis=1)
    )
    kernel_rows = (
        jnp.concatenate(
            [ahead_rows, jnp.zeros((per_device, 1), jnp.float32), jnp.flip(behind_rows[:, 1:], 1)],
            axis=1,
        )
        * norm_scale[:, None]
    )
    padded_length = 2 * seq_length
    height = padded_length // FACTOR
    tables = (
        phases(height, height, height)
        + phases(height, FACTOR, padded_length)
        + phases(FACTOR, FACTOR, FACTOR)
    )
    kernel_real, kernel_imag = forward_transform(
        kernel_rows.reshape(per_device, height, FACTOR), tables
    )
    signal_real, signal_imag = forward_transform(
        moved_signal.T.reshape(per_device, height // 2, FACTOR), tables
    )
    prod_real = signal_real * kernel_real - signal_imag * kernel_imag
    prod_imag = signal_real * kernel_imag + signal_imag * kernel_real
    response = inverse_transform(prod_real, prod_imag, tables, height // 2) / padded_length
    response = response.reshape(per_device, seq_length).T.astype(jnp.bfloat16)
    returned = lax.all_to_all(response, "row", split_axis=0, concat_axis=1, tiled=True)
    mixed_rows = (
        gate_part.astype(jnp.float32)
        * (returned.astype(jnp.float32) + skip_gain * signal.astype(jnp.float32))
    ).astype(jnp.bfloat16)
    whole_rows = lax.all_to_all(mixed_rows, "col", split_axis=0, concat_axis=1, tiled=True)
    return jnp.dot(whole_rows, output_weight, preferred_element_type=jnp.float32).astype(
        jnp.bfloat16
    )


WIDE = 256


def feature_table(seq_length):
    places = np.arange(seq_length, dtype=np.int64)
    bands = 1 + np.arange(BANDS, dtype=np.int64) * (seq_length // (4 * BANDS))
    angles = 2.0 * np.pi / seq_length * (places[:, None] * bands[None, :] % seq_length)
    scaled = places / (seq_length - 1)
    feats = np.concatenate([scaled[:, None], np.cos(angles), -np.sin(angles)], 1).astype(np.float32)
    high = feats.astype(jnp.bfloat16)
    low = (feats - high.astype(np.float32)).astype(jnp.bfloat16)
    used = np.zeros((seq_length, 128), jnp.bfloat16)
    count = feats.shape[1]
    for start, part in ((0, high), (40, low), (80, high)):
        used[:, start : start + count] = part
    used[:, 120:122] = 1
    return used


def sine_coefficients():
    u = 0.5 * np.cos(np.pi * (np.arange(4000) + 0.5) / 8000)
    powers = np.stack([u ** (2 * i + 1) for i in range(6)], 1)
    return [float(v) for v in np.linalg.lstsq(powers, np.sin(2 * np.pi * u), rcond=None)[0]]


SINE = sine_coefficients()
MAGIC = 12582912.0


def sine_of_turns(turns):
    u = turns - ((turns + MAGIC) - MAGIC)
    square = u * u
    total = SINE[-1]
    for value in SINE[-2::-1]:
        total = total * square + value
    return u * total


def split_two(value):
    high = value.astype(jnp.bfloat16)
    return high, (value - high.astype(jnp.float32)).astype(jnp.bfloat16)


def combine(terms):
    total = None
    for coef, array in terms:
        if abs(coef) < 1e-9:
            continue
        if abs(abs(coef) - 1.0) < 1e-9:
            if total is None:
                total = array if coef > 0 else -array
            else:
                total = total + array if coef > 0 else total - array
        else:
            total = array * coef if total is None else total + array * coef
    return total


def first_stage(planes):
    half = len(planes)
    full, mid = 2 * half, half // 2
    quarter = mid // 2
    theta = 2 * math.pi / full
    add = {r: planes[r] + planes[half - r] for r in range(1, mid)}
    sub = {r: planes[r] - planes[half - r] for r in range(1, mid)}
    add_add = {r: add[r] + add[mid - r] for r in range(1, quarter)}
    add_sub = {r: add[r] - add[mid - r] for r in range(1, quarter)}
    sub_add = {r: sub[r] + sub[mid - r] for r in range(1, quarter)}
    sub_sub = {r: sub[r] - sub[mid - r] for r in range(1, quarter)}
    ends = (planes[0] + planes[mid], planes[0] - planes[mid])
    out = []
    for k in range(half + 1):
        cos = lambda r: math.cos(theta * r * k)
        sin = lambda r: math.sin(theta * r * k)
        if k % 4 == 0:
            real = combine([(1.0, ends[0]), (cos(quarter), add[quarter])] + [(cos(r), add_add[r]) for r in add_add])
            imag = combine([(-sin(r), sub_sub[r]) for r in sub_sub])
        elif k % 2 == 0:
            real = combine([(1.0, ends[1])] + [(cos(r), add_sub[r]) for r in add_sub])
            imag = combine([(-sin(quarter), sub[quarter])] + [(-sin(r), sub_add[r]) for r in sub_add])
        else:
            real = combine([(1.0, planes[0])] + [(cos(r), sub[r]) for r in sub])
            imag = combine([(-sin(mid), planes[mid])] + [(-sin(r), add[r]) for r in add])
        out.append((real, imag))
    return out


def last_stage(pairs):
    half = len(pairs) - 1
    full, mid = 2 * half, half // 2
    quarter = mid // 2
    theta = 2 * math.pi / full
    four = range(0, half + 1, 4)
    two = range(2, half + 1, 4)
    odd = range(1, half + 1, 2)
    real = [p[0] for p in pairs]
    imag = [p[1] for p in pairs]
    out = [None] * half

    def cosines(r, ks):
        return combine([(math.cos(theta * r * k), real[k]) for k in ks])

    def sines(r, ks):
        return combine([(math.sin(theta * r * k), imag[k]) for k in ks])

    out[0] = combine([(1.0, v) for v in real])
    out[mid] = cosines(mid, list(four) + list(two)) - sines(mid, odd)

    def place(r, cos_even, sin_even):
        cos_odd, sin_odd = cosines(r, odd), sines(r, odd)
        out[r] = (cos_even - sin_even) + (cos_odd - sin_odd)
        out[half - r] = (cos_even + sin_even) - (cos_odd + sin_odd)

    for r in range(1, quarter):
        c0, c2, s0, s2 = cosines(r, four), cosines(r, two), sines(r, four), sines(r, two)
        place(r, c0 + c2, s0 + s2)
        place(mid - r, c0 - c2, s2 - s0)
    place(quarter, cosines(quarter, four), sines(quarter, two))
    return out


def tiles(count, body):
    lanes = WIDE // 128

    def one(i, carry):
        body(pl.multiple_of(i // lanes * 16, 16), pl.multiple_of(i % lanes * 128, 128))
        return carry

    lax.fori_loop(0, count // 16 * lanes, one, 0)


def layer_kernel(
    tokens_h, outer_h, inner_h, value_h, out_weight_h, feats_h,
    taps, feature_weight, feature_phase, inner_mats, inner_phase, frequency, forward, backward, rate, skip,
    twist_c, twist_s, cos_t, sin_t,
    out_ref,
    tok, weights, out_weight, feats, sig_send, sig_recv, resp_send, resp_recv, mix_send, mix_recv,
    sums, diffs, turned, filt, back, scale_ref, first_ref, chan, rate_col, energy_ref, gate_ref, signal_ref,
    local_sem, edge_send, edge_recv, sig_s, sig_r, resp_s, resp_r, mix_s, mix_r,
):
    f32, bf16 = jnp.float32, jnp.bfloat16
    dot = functools.partial(jnp.dot, preferred_element_type=f32)
    n_row, n_col = lax.axis_size("row"), lax.axis_size("col")
    row, col = lax.axis_index("row"), lax.axis_index("col")
    length, rows = feats.shape[0], tokens_h.shape[0]
    width = outer_h.shape[1]
    count = width // n_row
    planes = length // WIDE
    per = rows // WIDE
    mesh_id = pl.DeviceIdType.MESH

    barrier = pltpu.get_barrier_semaphore()
    for o in range(1, n_row):
        pl.semaphore_signal(barrier, inc=1, device_id=(lax.rem(row + o, n_row), col), device_id_type=mesh_id)
    for o in range(1, n_col):
        pl.semaphore_signal(barrier, inc=1, device_id=(row, lax.rem(col + o, n_col)), device_id_type=mesh_id)
    loads = [
        pltpu.make_async_copy(feats_h, feats, local_sem.at[0]),
        pltpu.make_async_copy(tokens_h, tok.at[pl.ds(0, rows)], local_sem.at[1]),
        pltpu.make_async_copy(inner_h, weights.at[1], local_sem.at[2]),
        pltpu.make_async_copy(value_h, weights.at[2], local_sem.at[3]),
        pltpu.make_async_copy(outer_h, weights.at[0], local_sem.at[4]),
        pltpu.make_async_copy(out_weight_h, out_weight, local_sem.at[5]),
    ]
    for load in loads:
        load.start()

    turn = frequency[...] * (0.5 / math.pi)
    high, low = split_two(feature_weight[...] * turn)
    phase_high, phase_low = split_two(feature_phase[...] * turn)
    used = high.shape[0]
    first_ref[...] = jnp.zeros_like(first_ref)
    first_ref[0:used] = high.astype(f32)
    first_ref[40 : 40 + used] = high.astype(f32)
    first_ref[80 : 80 + used] = low.astype(f32)
    first_ref[120:121] = phase_high.astype(f32)
    first_ref[121:122] = phase_low.astype(f32)
    first_w = first_ref[...].astype(bf16)
    inner_w = []
    for level in range(INNER):
        mat_high, mat_low = split_two(inner_mats[level] * turn)
        inner_w.append(jnp.concatenate([
            jnp.concatenate([mat_high, mat_low], 1), jnp.concatenate([mat_high, jnp.zeros_like(mat_low)], 1)], 0))
    inner_p = inner_phase[...] * turn
    chan[0] = forward[...].T
    chan[1] = backward[...].T
    rate_col[...] = jnp.broadcast_to(rate[...], (128, width)).T
    own = pl.ds(pl.multiple_of(row * count, 16), count)
    both_w = jnp.concatenate([chan[0, own, :], chan[1, own, :]], 0).astype(bf16)
    rates = rate_col[own, 0:1]
    chunk = 512
    energy_ref[...] = jnp.zeros_like(energy_ref)

    def one_chunk(i, carry):
        at = pl.ds(pl.multiple_of(i * chunk, chunk), chunk)
        hidden = sine_of_turns(dot(feats[at, :], first_w))
        for level in range(INNER):
            h_high, h_low = split_two(hidden)
            wide = dot(jnp.concatenate([h_high, h_low], 1), inner_w[level])
            hidden = sine_of_turns(wide[:, :128] + wide[:, 128:] + inner_p[level : level + 1, :])
        both = lax.dot_general(both_w, hidden.astype(bf16), (((1,), (1,)), ((), ())), preferred_element_type=f32)
        place = lax.broadcasted_iota(jnp.int32, (count, chunk), 1) + i * chunk
        window = jnp.exp(place.astype(f32) * (-1.0 / (length - 1)) * rates)
        ahead = both[:count] * window
        behind = jnp.where(place == 0, 0.0, both[count:] * window)
        sums[:, at] = ahead + behind
        diffs[:, at] = ahead - behind
        energy_ref[...] += jnp.broadcast_to(
            jnp.sum(ahead * ahead + behind * behind, axis=1, keepdims=True), (count, 128))
        return carry

    early = min(EARLY, length // chunk)
    loads[0].wait()
    lax.fori_loop(0, early, one_chunk, 0)

    pl.semaphore_wait(barrier, n_row + n_col - 2)
    edges = [
        pltpu.make_async_remote_copy(
            src_ref=tokens_h.at[pl.ds(rows - 16 if i == 0 else 0, 16)],
            dst_ref=tok.at[pl.ds(rows + 16 * i, 16)],
            send_sem=edge_send.at[i], recv_sem=edge_recv.at[i],
            device_id=(lax.rem(row + (1 if i == 0 else n_row - 1), n_row), col), device_id_type=mesh_id)
        for i in range(2)
    ]
    for edge in edges:
        edge.start()
    loads[1].wait()
    loads[2].wait()
    loads[3].wait()
    for edge in edges:
        edge.wait()

    index = lax.broadcasted_iota(jnp.int32, (rows, width), 0)
    has_before = jnp.where(row > 0, 1.0, 0.0)
    has_after = jnp.where(row < n_row - 1, 1.0, 0.0)

    def convolved(j):
        proj = dot(tok[...], weights[j]).astype(bf16).astype(f32)
        main = proj[:rows]
        first = proj[rows + 15 : rows + 16] * has_before
        last = proj[rows + 16 : rows + 17] * has_after
        before = jnp.where(index == 0, first, pltpu.roll(main, 1, 0))
        after = jnp.where(index == rows - 1, last, pltpu.roll(main, rows - 1, 0))
        return before * taps[0, j : j + 1, :] + main * taps[1, j : j + 1, :] + after * taps[2, j : j + 1, :]

    signal = (convolved(1) * convolved(2)).astype(bf16)
    signal_ref[...] = signal
    flipped = signal.astype(f32).T.astype(bf16)
    for g in range(n_row):
        sig_send[g] = flipped[g * count : (g + 1) * count]

    def exchange(send, recv, s_sem, r_sem, size, me, target):
        copies = []
        for o in range(1, size):
            peer = lax.rem(me + o, size)
            copies.append(pltpu.make_async_remote_copy(
                src_ref=send.at[peer], dst_ref=recv.at[me],
                send_sem=s_sem.at[o], recv_sem=r_sem.at[o], device_id=target(peer), device_id_type=mesh_id))
        for copy in copies:
            copy.start()
        recv[me] = send[me]
        return copies

    along_row = lambda peer: (peer, col)
    along_col = lambda peer: (row, peer)
    travelling = exchange(sig_send, sig_recv, sig_s, sig_r, n_row, row, along_row)

    loads[4].wait()
    gate_ref[...] = convolved(0).astype(bf16)
    lax.fori_loop(early, length // chunk, one_chunk, 0)
    scale_ref[...] = lax.rsqrt(1.0 + energy_ref[...]) * (0.5 / length)

    def turn_into(first, pairs, top, left, weighted):
        for k, (real, imag) in enumerate(pairs):
            c, s = twist_c[k : k + 1, pl.ds(left, 128)], twist_s[k : k + 1, pl.ds(left, 128)]
            if weighted and k not in (0, planes):
                c, s = c * 2.0, s * 2.0
            at = pl.ds(pl.multiple_of(k * count + top, 16), 16)
            if imag is None:
                new_real, new_imag = real * c, -(real * s)
            else:
                new_real, new_imag = real * c + imag * s, imag * c - real * s
            turned[first, at, pl.ds(left, 128)] = new_real.astype(bf16)
            turned[first + 1, at, pl.ds(left, 128)] = new_imag.astype(bf16)

    def filter_tile(top, left):
        scale = scale_ref[pl.ds(top, 16), :]
        for which, source in enumerate((sums, diffs)):
            got = [source[pl.ds(top, 16), pl.ds(pl.multiple_of(r * WIDE + left, 128), 128)] * scale for r in range(planes)]
            turn_into(2 * which, first_stage(got), top, left, True)

    tiles(count, filter_tile)
    filt[0] = dot(turned[0], cos_t[...]) + dot(turned[1], sin_t[...])
    filt[1] = dot(turned[3], cos_t[...]) - dot(turned[2], sin_t[...])
    for copy in travelling:
        copy.wait()

    def signal_tile(top, left):
        got = [sig_recv[r // per, pl.ds(top, 16), pl.ds(pl.multiple_of(r % per * WIDE + left, 128), 128)].astype(f32)
               for r in range(planes)]
        turn_into(0, first_stage(got), top, left, False)

    tiles(count, signal_tile)
    real = dot(turned[0], cos_t[...]) + dot(turned[1], sin_t[...])
    imag = dot(turned[1], cos_t[...]) - dot(turned[0], sin_t[...])
    prod_real = (real * filt[0] - imag * filt[1]).astype(bf16)
    prod_imag = (real * filt[1] + imag * filt[0]).astype(bf16)
    back[0] = dot(prod_real, cos_t[...]) - dot(prod_imag, sin_t[...])
    back[1] = dot(prod_imag, cos_t[...]) + dot(prod_real, sin_t[...])

    def back_tile(top, left):
        pairs = []
        for k in range(planes + 1):
            c, s = twist_c[k : k + 1, pl.ds(left, 128)], twist_s[k : k + 1, pl.ds(left, 128)]
            at = pl.ds(pl.multiple_of(k * count + top, 16), 16)
            b_real, b_imag = back[0, at, pl.ds(left, 128)], back[1, at, pl.ds(left, 128)]
            pairs.append((b_real * c - b_imag * s, b_imag * c + b_real * s))
        for r, plane in enumerate(last_stage(pairs)):
            at = pl.multiple_of(r % per * WIDE + left, 128)
            resp_send[r // per, pl.ds(top, 16), pl.ds(at, 128)] = plane.astype(bf16)

    tiles(count, back_tile)
    for copy in exchange(resp_send, resp_recv, resp_s, resp_r, n_row, row, along_row):
        copy.wait()
    response = jnp.concatenate([resp_recv[g].astype(f32) for g in range(n_row)], 0).T
    mixed = (gate_ref[...].astype(f32) * (response + skip[...] * signal_ref[...].astype(f32))).astype(bf16)
    share = rows // n_col
    for p in range(n_col):
        mix_send[p] = mixed[p * share : (p + 1) * share]
    travelling = exchange(mix_send, mix_recv, mix_s, mix_r, n_col, col, along_col)
    loads[5].wait()
    for copy in travelling:
        copy.wait()
    left_side = jnp.concatenate([mix_recv[p] for p in range(n_col)], 1)
    out_width = out_ref.shape[1]
    for j in range(0, out_width, 512):
        out_ref[:, j : j + 512] = dot(left_side, out_weight[:, j : j + 512]).astype(bf16)


EARLY = 2


def fits(tokens_rows, seq_length, own_width, row_devices, units):
    planes = seq_length // WIDE
    members = own_width // row_devices
    return (
        own_width % 128 == 0
        and members % 16 == 0
        and tokens_rows % WIDE == 0
        and seq_length % 512 == 0
        and planes % 8 == 0
        and 8 <= planes <= 32
        and units == 128
        and tokens_rows % 64 == 0
    )


def on_device_fast(
    tokens, outer_weight, inner_weight, value_weight, conv_taps, feature_weight, feature_phase,
    inner_mats, inner_phase, frequency, forward_weight, backward_weight, decay_rate, skip_gain, output_weight,
):
    f32, bf16 = jnp.float32, jnp.bfloat16
    rows, depth = tokens.shape
    devices = lax.axis_size("row")
    seq_length = rows * devices
    width = outer_weight.shape[1]
    members = width // devices
    planes = seq_length // WIDE
    n_col = lax.axis_size("col")
    k_index = np.arange(planes + 1)[:, None] * np.arange(WIDE)[None, :]
    twist_c = jnp.asarray(np.cos(2 * np.pi * k_index / (2 * seq_length)), f32)
    twist_s = jnp.asarray(np.sin(2 * np.pi * k_index / (2 * seq_length)), f32)
    w_index = np.arange(WIDE)[:, None] * np.arange(WIDE)[None, :] % WIDE
    cos_t = jnp.asarray(np.cos(2 * np.pi * w_index / WIDE), bf16)
    sin_t = jnp.asarray(np.sin(2 * np.pi * w_index / WIDE), bf16)
    spec_rows = (planes + 1) * members
    any_spec = pl.BlockSpec(memory_space=pl.ANY)
    vmem = pl.BlockSpec(memory_space=pltpu.VMEM)
    dma = pltpu.SemaphoreType.DMA
    share = rows // n_col
    out_width = output_weight.shape[1]
    exchanged = pltpu.VMEM((devices, members, rows), bf16)
    spread = pltpu.VMEM((n_col, share, width), bf16)
    return pl.pallas_call(
        layer_kernel,
        out_shape=jax.ShapeDtypeStruct((share, out_width), bf16),
        in_specs=[any_spec] * 6 + [vmem] * 14,
        out_specs=vmem,
        scratch_shapes=[
            pltpu.VMEM((rows + 32, depth), bf16),
            pltpu.VMEM((3, depth, width), bf16),
            pltpu.VMEM(output_weight.shape, bf16),
            pltpu.VMEM((seq_length, 128), bf16),
            exchanged, exchanged, exchanged, exchanged, spread, spread,
            pltpu.VMEM((members, seq_length), f32),
            pltpu.VMEM((members, seq_length), f32),
            pltpu.VMEM((4, spec_rows, WIDE), bf16),
            pltpu.VMEM((2, spec_rows, WIDE), f32),
            pltpu.VMEM((2, spec_rows, WIDE), f32),
            pltpu.VMEM((members, 128), f32),
            pltpu.VMEM((128, 128), f32),
            pltpu.VMEM((2, width, 128), f32),
            pltpu.VMEM((width, 128), f32),
            pltpu.VMEM((members, 128), f32),
            pltpu.VMEM((rows, width), bf16),
            pltpu.VMEM((rows, width), bf16),
            dma((6,)), dma((2,)), dma((2,)),
            dma((devices,)), dma((devices,)), dma((devices,)), dma((devices,)), dma((n_col,)), dma((n_col,)),
        ],
        compiler_params=pltpu.CompilerParams(
            collective_id=0, has_side_effects=True, vmem_limit_bytes=56 * 1024 * 1024),
        name="layer",
    )(
        tokens, outer_weight, inner_weight, value_weight, output_weight, jnp.asarray(feature_table(seq_length)),
        conv_taps, feature_weight, feature_phase[None], inner_mats, inner_phase, frequency[None],
        forward_weight, backward_weight, decay_rate[None], skip_gain[None], twist_c, twist_s, cos_t, sin_t,
    )


def on_any(*args):
    tokens, outer_weight, feature_weight = args[0], args[1], args[5]
    devices = lax.axis_size("row")
    if fits(tokens.shape[0], tokens.shape[0] * devices, outer_weight.shape[1], devices, feature_weight.shape[1]):
        return on_device_fast(*args)
    return on_device(*args)


def solution(mesh):
    placed = (
        P("row", None),
        P(None, "col"),
        P(None, "col"),
        P(None, "col"),
        P(None, None, "col"),
        P(),
        P(),
        P(),
        P(),
        P(),
        P(None, "col"),
        P(None, "col"),
        P("col"),
        P("col"),
        P(),
    )
    return jax.shard_map(
        on_any, mesh=mesh, in_specs=placed, out_specs=P(("row", "col"), None), check_vma=False
    )
```

profile of v0, /device:TPU:0, one launch (start us, length us, event | category | flops | bytes accessed | tf_op | source)
XLA Modules:
  0.0 38.3 jit_solution(12533033728830913554)
XLA Ops:
  0.0 36.4 %layer.1 = bf16[128,2048]{1,0:T(8,128)(2,1)} custom-call(bf16[512,2048]{1,0:T(8,128)(2,1)} %tokens_h.1, bf16[2048,256]{1,0:T(8,128)(2,1)} %outer_h.1, bf16[2048,256]{1,0:T(8,128)(2,1)} %inner_h.1, bf16[2048,256]{1,0:T(8,128)(2,1)} %value_h.1, bf16[1024,2048]{1,0:T(8,128)(2,1)} %out_weight_h.1, bf16[4096,128]{1,0:T(8,128)(2,1)} %constant.14.clone.feats_h, ...), custom_call_target="tpu_custom_call" | custom-call | tf_op jit(solution)/shard_map/layer/pallas_call | solution.py:583
  36.4 1.9 %copy.22 = bf16[128,2048]{1,0:T(8,128)(2,1)} copy(bf16[128,2048]{1,0:T(8,128)(2,1)} %layer.1) | data formatting | bytes 1048576
where the time goes:
time: 38.6 us; the launch traced here: 38.3 us
  Pallas kernels  36.4 us (94%)
  local copies, waits for them, and re-layouts  1.88 us (5%)
    pallas_call x1, Pallas kernels, on_device_fast(): pl.pallas_call(layer_kernel, out_shape=jax.ShapeDtypeStruct((share, out_w...  36.4 us
    unnamed x1, local copies, waits for them, and re-layouts  1.88 us

commit v1 on v0

--- a/solution.py
+++ b/solution.py
@@ -329,19 +329,20 @@
 
 
 def layer_kernel(
-    tokens_h, outer_h, inner_h, value_h, out_weight_h, feats_h,
+    tokens_h, outer_h, inner_h, value_h, feats_h,
     taps, feature_weight, feature_phase, inner_mats, inner_phase, frequency, forward, backward, rate, skip,
     twist_c, twist_s, cos_t, sin_t,
     out_ref,
-    tok, weights, out_weight, feats, sig_send, sig_recv, resp_send, resp_recv, mix_send, mix_recv,
+    tok, weights, feats, hid, sig_send, sig_recv, resp_send, resp_recv, mix_send, mix_recv,
     sums, diffs, turned, filt, back, scale_ref, first_ref, chan, rate_col, energy_ref, gate_ref, signal_ref,
-    local_sem, edge_send, edge_recv, sig_s, sig_r, resp_s, resp_r, mix_s, mix_r,
+    local_sem, edge_send, edge_recv, hid_s, hid_r, sig_s, sig_r, resp_s, resp_r, mix_s, mix_r,
 ):
     f32, bf16 = jnp.float32, jnp.bfloat16
     dot = functools.partial(jnp.dot, preferred_element_type=f32)
     n_row, n_col = lax.axis_size("row"), lax.axis_size("col")
     row, col = lax.axis_index("row"), lax.axis_index("col")
-    length, rows = feats.shape[0], tokens_h.shape[0]
+    length, rows = feats_h.shape[0], tokens_h.shape[0]
+    quarter = length // n_col
     width = outer_h.shape[1]
     count = width // n_row
     planes = length // WIDE
@@ -354,12 +355,12 @@
     for o in range(1, n_col):
         pl.semaphore_signal(barrier, inc=1, device_id=(row, lax.rem(col + o, n_col)), device_id_type=mesh_id)
     loads = [
-        pltpu.make_async_copy(feats_h, feats, local_sem.at[0]),
+        pltpu.make_async_copy(
+            feats_h.at[pl.ds(pl.multiple_of(col * quarter, 512), quarter)], feats, local_sem.at[0]),
         pltpu.make_async_copy(tokens_h, tok.at[pl.ds(0, rows)], local_sem.at[1]),
         pltpu.make_async_copy(inner_h, weights.at[1], local_sem.at[2]),
         pltpu.make_async_copy(value_h, weights.at[2], local_sem.at[3]),
         pltpu.make_async_copy(outer_h, weights.at[0], local_sem.at[4]),
-        pltpu.make_async_copy(out_weight_h, out_weight, local_sem.at[5]),
     ]
     for load in loads:
         load.start()
@@ -390,15 +391,20 @@
     chunk = 512
     energy_ref[...] = jnp.zeros_like(energy_ref)
 
-    def one_chunk(i, carry):
-        at = pl.ds(pl.multiple_of(i * chunk, chunk), chunk)
+    def hidden_chunk(i):
+        at = pl.ds(i * chunk, chunk)
         hidden = sine_of_turns(dot(feats[at, :], first_w))
         for level in range(INNER):
             h_high, h_low = split_two(hidden)
             wide = dot(jnp.concatenate([h_high, h_low], 1), inner_w[level])
             hidden = sine_of_turns(wide[:, :128] + wide[:, 128:] + inner_p[level : level + 1, :])
-        both = lax.dot_general(both_w, hidden.astype(bf16), (((1,), (1,)), ((), ())), preferred_element_type=f32)
-        place = lax.broadcasted_iota(jnp.int32, (count, chunk), 1) + i * chunk
+        hid[col, at, :] = hidden.astype(bf16)
+
+    def filter_chunk(owner, i):
+        at = pl.ds(pl.multiple_of(owner * quarter + i * chunk, chunk), chunk)
+        both = lax.dot_general(both_w, hid[owner, pl.ds(i * chunk, chunk), :], (((1,), (1,)), ((), ())),
+                               preferred_element_type=f32)
+        place = lax.broadcasted_iota(jnp.int32, (count, chunk), 1) + (owner * quarter + i * chunk)
         window = jnp.exp(place.astype(f32) * (-1.0 / (length - 1)) * rates)
         ahead = both[:count] * window
         behind = jnp.where(place == 0, 0.0, both[count:] * window)
@@ -406,11 +412,20 @@
         diffs[:, at] = ahead - behind
         energy_ref[...] += jnp.broadcast_to(
             jnp.sum(ahead * ahead + behind * behind, axis=1, keepdims=True), (count, 128))
-        return carry
-
-    early = min(EARLY, length // chunk)
+
+    pieces = quarter // chunk
+    partner = col + 1 - 2 * lax.rem(col, 2)
+    across = lax.rem(col + 2, n_col)
+
+    def pass_on(kind, owner, i, target):
+        part = hid.at[owner, pl.ds(i * chunk, chunk)]
+        return pltpu.make_async_remote_copy(
+            src_ref=part, dst_ref=part, send_sem=hid_s.at[kind, i], recv_sem=hid_r.at[kind, i],
+            device_id=(row, target), device_id_type=mesh_id)
+
     loads[0].wait()
-    lax.fori_loop(0, early, one_chunk, 0)
+    for i in range(pieces):
+        hidden_chunk(i)
 
     pl.semaphore_wait(barrier, n_row + n_col - 2)
     edges = [
@@ -423,6 +438,11 @@
     ]
     for edge in edges:
         edge.start()
+    to_across = [pass_on(0, col, i, across) for i in range(pieces)]
+    to_partner = [pass_on(1, col, i, partner) for i in range(pieces)]
+    relayed = [pass_on(2, across, i, partner) for i in range(pieces)]
+    for copy in to_across + to_partner:
+        copy.start()
     loads[1].wait()
     loads[2].wait()
     loads[3].wait()
@@ -466,7 +486,19 @@
 
     loads[4].wait()
     gate_ref[...] = convolved(0).astype(bf16)
-    lax.fori_loop(early, length // chunk, one_chunk, 0)
+    for i in range(pieces):
+        filter_chunk(col, i)
+    for i in range(pieces):
+        to_partner[i].wait()
+        filter_chunk(partner, i)
+    for i in range(pieces):
+        to_across[i].wait()
+        relayed[i].start()
+    for i in range(pieces):
+        filter_chunk(across, i)
+    for i in range(pieces):
+        relayed[i].wait()
+        filter_chunk(lax.rem(partner + 2, n_col), i)
     scale_ref[...] = lax.rsqrt(1.0 + energy_ref[...]) * (0.5 / length)
 
     def turn_into(first, pairs, top, left, weighted):
@@ -527,19 +559,13 @@
     for p in range(n_col):
         mix_send[p] = mixed[p * share : (p + 1) * share]
     travelling = exchange(mix_send, mix_recv, mix_s, mix_r, n_col, col, along_col)
-    loads[5].wait()
     for copy in travelling:
         copy.wait()
-    left_side = jnp.concatenate([mix_recv[p] for p in range(n_col)], 1)
-    out_width = out_ref.shape[1]
-    for j in range(0, out_width, 512):
-        out_ref[:, j : j + 512] = dot(left_side, out_weight[:, j : j + 512]).astype(bf16)
-
-
-EARLY = 2
-
-
-def fits(tokens_rows, seq_length, own_width, row_devices, units):
+    for p in range(n_col):
+        out_ref[:, p * width : (p + 1) * width] = mix_recv[p]
+
+
+def fits(tokens_rows, seq_length, own_width, row_devices, col_devices, units):
     planes = seq_length // WIDE
     members = own_width // row_devices
     return (
@@ -551,6 +577,8 @@
         and 8 <= planes <= 32
         and units == 128
         and tokens_rows % 64 == 0
+        and col_devices == 4
+        and seq_length % 2048 == 0
     )
 
 
@@ -577,19 +605,19 @@
     vmem = pl.BlockSpec(memory_space=pltpu.VMEM)
     dma = pltpu.SemaphoreType.DMA
     share = rows // n_col
-    out_width = output_weight.shape[1]
+    pieces = seq_length // n_col // 512
     exchanged = pltpu.VMEM((devices, members, rows), bf16)
     spread = pltpu.VMEM((n_col, share, width), bf16)
-    return pl.pallas_call(
+    mixed = pl.pallas_call(
         layer_kernel,
-        out_shape=jax.ShapeDtypeStruct((share, out_width), bf16),
-        in_specs=[any_spec] * 6 + [vmem] * 14,
+        out_shape=jax.ShapeDtypeStruct((share, n_col * width), bf16),
+        in_specs=[any_spec] * 5 + [vmem] * 14,
         out_specs=vmem,
         scratch_shapes=[
             pltpu.VMEM((rows + 32, depth), bf16),
             pltpu.VMEM((3, depth, width), bf16),
-            pltpu.VMEM(output_weight.shape, bf16),
-            pltpu.VMEM((seq_length, 128), bf16),
+            pltpu.VMEM((seq_length // n_col, 128), bf16),
+            pltpu.VMEM((n_col, seq_length // n_col, 128), bf16),
             exchanged, exchanged, exchanged, exchanged, spread, spread,
             pltpu.VMEM((members, seq_length), f32),
             pltpu.VMEM((members, seq_length), f32),
@@ -603,23 +631,27 @@
             pltpu.VMEM((members, 128), f32),
             pltpu.VMEM((rows, width), bf16),
             pltpu.VMEM((rows, width), bf16),
-            dma((6,)), dma((2,)), dma((2,)),
+            dma((5,)), dma((2,)), dma((2,)), dma((3, pieces)), dma((3, pieces)),
             dma((devices,)), dma((devices,)), dma((devices,)), dma((devices,)), dma((n_col,)), dma((n_col,)),
         ],
         compiler_params=pltpu.CompilerParams(
-            collective_id=0, has_side_effects=True, vmem_limit_bytes=56 * 1024 * 1024),
+            collective_id=0, has_side_effects=True, vmem_limit_bytes=GRANT),
         name="layer",
     )(
-        tokens, outer_weight, inner_weight, value_weight, output_weight, jnp.asarray(feature_table(seq_length)),
+        tokens, outer_weight, inner_weight, value_weight, jnp.asarray(feature_table(seq_length)),
         conv_taps, feature_weight, feature_phase[None], inner_mats, inner_phase, frequency[None],
         forward_weight, backward_weight, decay_rate[None], skip_gain[None], twist_c, twist_s, cos_t, sin_t,
     )
+    return jnp.dot(mixed, output_weight, preferred_element_type=f32).astype(bf16)
+
+
+GRANT = 54 * 1024 * 1024
 
 
 def on_any(*args):
     tokens, outer_weight, feature_weight = args[0], args[1], args[5]
     devices = lax.axis_size("row")
-    if fits(tokens.shape[0], tokens.shape[0] * devices, outer_weight.shape[1], devices, feature_weight.shape[1]):
+    if fits(tokens.shape[0], tokens.shape[0] * devices, outer_weight.shape[1], devices, lax.axis_size("col"), feature_weight.shape[1]):
         return on_device_fast(*args)
     return on_device(*args)
 

time: 38.6 us -> 36.6 us (0.948)
  Pallas kernels: 36.4 us -> 33.9 us
  matrix products: 0 us -> 2.47 us
  local copies, waits for them, and re-layouts: 1.88 us -> 0.01 us
    pallas_call x1, Pallas kernels: 36.4 us -> 33.9 us  [on_device_fast(): pl.pallas_call(layer_kernel, out_shape=jax.ShapeDtypeStruct((share, n_col...]
    dot_general x0 -> x1, matrix products: none -> 2.47 us  [on_device_fast(): jnp.dot(mixed, output_weight, preferred_element_type=f32).astype(bf16)]
    unnamed x1 -> x2, local copies, waits for them, and re-layouts: 1.88 us -> 0.01 us
where the time goes in v1:
time: 36.6 us; the launch traced here: 36.4 us
  Pallas kernels  33.9 us (93%)
  matrix products  2.47 us (7%)
    pallas_call x1, Pallas kernels, on_device_fast(): pl.pallas_call(layer_kernel, out_shape=jax.ShapeDtypeStruct((share, n_col...  33.9 us
    dot_general x1, matrix products, on_device_fast(): jnp.dot(mixed, output_weight, preferred_element_type=f32).astype(bf16)  2.47 us

profile of v1, /device:TPU:0, one launch (start us, length us, event | category | flops | bytes accessed | tf_op | source)
XLA Modules:
  0.0 36.4 jit_solution(11296561609518672340)
XLA Ops:
  0.0 0.0 copy-start
  0.0 33.9 %layer.1 = bf16[128,1024]{1,0:T(8,128)(2,1)} custom-call(bf16[512,2048]{1,0:T(8,128)(2,1)} %tokens_h.1, bf16[2048,256]{1,0:T(8,128)(2,1)} %outer_h.1, bf16[2048,256]{1,0:T(8,128)(2,1)} %inner_h.1, bf16[2048,256]{1,0:T(8,128)(2,1)} %value_h.1, bf16[4096,128]{1,0:T(8,128)(2,1)} %constant.14.clone.feats_h, f32[3,3,256]{2,1,0:T(4,128)} %taps.1, ...), custom_call_target="tpu_custom_call" | custom-call | tf_op jit(solution)/shard_map/layer/pallas_call | solution.py:611
  33.9 0.0 copy-done
  33.9 2.5 %convolution_convert_fusion = bf16[128,2048]{1,0:T(8,128)(2,1)} fusion(bf16[128,1024]{1,0:T(8,128)(2,1)} %layer.1, bf16[1024,2048]{1,0:T(8,128)(2,1)S(1)} %copy-done), kind=kOutput, calls=%fused_computation | convolution fusion | flops 537133056 | bytes 4980736 | tf_op jit(solution)/shard_map/dot_general | solution.py:645
Async XLA Ops:
  0.0 33.9 %copy-start = (bf16[1024,2048]{1,0:T(8,128)(2,1)S(1)}, bf16[1024,2048]{1,0:T(8,128)(2,1)}, u32[]{:S(2)}) copy-start(bf16[1024,2048]{1,0:T(8,128)(2,1)} %param.34) | copy-start | bytes 12582916

commit v2 on v1

--- a/solution.py
+++ b/solution.py
@@ -550,8 +550,22 @@
             at = pl.multiple_of(r % per * WIDE + left, 128)
             resp_send[r // per, pl.ds(top, 16), pl.ds(at, 128)] = plane.astype(bf16)
 
-    tiles(count, back_tile)
-    for copy in exchange(resp_send, resp_recv, resp_s, resp_r, n_row, row, along_row):
+    def back_step(top, i, carry):
+        back_tile(top, pl.multiple_of(i * 128, 128))
+        return carry
+
+    travelling = []
+    for h in range(count // 16):
+        lax.fori_loop(0, WIDE // 128, functools.partial(back_step, h * 16), 0)
+        for o in range(1, n_row):
+            peer = lax.rem(row + o, n_row)
+            travelling.append(pltpu.make_async_remote_copy(
+                src_ref=resp_send.at[peer, pl.ds(h * 16, 16)], dst_ref=resp_recv.at[row, pl.ds(h * 16, 16)],
+                send_sem=resp_s.at[h, o], recv_sem=resp_r.at[h, o],
+                device_id=along_row(peer), device_id_type=mesh_id))
+            travelling[-1].start()
+    resp_recv[row] = resp_send[row]
+    for copy in travelling:
         copy.wait()
     response = jnp.concatenate([resp_recv[g].astype(f32) for g in range(n_row)], 0).T
     mixed = (gate_ref[...].astype(f32) * (response + skip[...] * signal_ref[...].astype(f32))).astype(bf16)
@@ -632,7 +646,7 @@
             pltpu.VMEM((rows, width), bf16),
             pltpu.VMEM((rows, width), bf16),
             dma((5,)), dma((2,)), dma((2,)), dma((3, pieces)), dma((3, pieces)),
-            dma((devices,)), dma((devices,)), dma((devices,)), dma((devices,)), dma((n_col,)), dma((n_col,)),
+            dma((devices,)), dma((devices,)), dma((members // 16, devices)), dma((members // 16, devices)), dma((n_col,)), dma((n_col,)),
         ],
         compiler_params=pltpu.CompilerParams(
             collective_id=0, has_side_effects=True, vmem_limit_bytes=GRANT),

time: 36.6 us -> 36.9 us (level)
  Pallas kernels: 33.9 us -> 34.3 us
where the time goes in v2:
time: 36.9 us; the launch traced here: 36.8 us
  Pallas kernels  34.3 us (93%)
  matrix products  2.46 us (7%)
    pallas_call x1, Pallas kernels, on_device_fast(): pl.pallas_call(layer_kernel, out_shape=jax.ShapeDtypeStruct((share, n_col...  34.3 us
    dot_general x1, matrix products, on_device_fast(): jnp.dot(mixed, output_weight, preferred_element_type=f32).astype(bf16)  2.46 us

profile of v2, /device:TPU:0, one launch (start us, length us, event | category | flops | bytes accessed | tf_op | source)
XLA Modules:
  0.0 36.8 jit_solution(6663396749603074882)
XLA Ops:
  0.0 0.0 copy-start
  0.0 34.3 %layer.1 = bf16[128,1024]{1,0:T(8,128)(2,1)} custom-call(bf16[512,2048]{1,0:T(8,128)(2,1)} %tokens_h.1, bf16[2048,256]{1,0:T(8,128)(2,1)} %outer_h.1, bf16[2048,256]{1,0:T(8,128)(2,1)} %inner_h.1, bf16[2048,256]{1,0:T(8,128)(2,1)} %value_h.1, bf16[4096,128]{1,0:T(8,128)(2,1)} %constant.14.clone.feats_h, f32[3,3,256]{2,1,0:T(4,128)} %taps.1, ...), custom_call_target="tpu_custom_call" | custom-call | tf_op jit(solution)/shard_map/layer/pallas_call | solution.py:625
  34.3 0.0 copy-done
  34.3 2.5 %convolution_convert_fusion = bf16[128,2048]{1,0:T(8,128)(2,1)} fusion(bf16[128,1024]{1,0:T(8,128)(2,1)} %layer.1, bf16[1024,2048]{1,0:T(8,128)(2,1)S(1)} %copy-done), kind=kOutput, calls=%fused_computation | convolution fusion | flops 537133056 | bytes 4980736 | tf_op jit(solution)/shard_map/dot_general | solution.py:659
Async XLA Ops:
  0.0 34.3 %copy-start = (bf16[1024,2048]{1,0:T(8,128)(2,1)S(1)}, bf16[1024,2048]{1,0:T(8,128)(2,1)}, u32[]{:S(2)}) copy-start(bf16[1024,2048]{1,0:T(8,128)(2,1)} %param.34) | copy-start | bytes 12582916
